TPU v7x, 256 devices: a 8x8x2 block of a 8x8x16 slice. The times are simulated.
256 devices in a mesh: grp: 2 (over z), sp: 64 (over y, x), tp: 2 (over core).
Axes of the slice: x: 8, y: 8, z: 2, core: 2. Of those that a mesh axis runs over, the one named last changes fastest.
The devices are a block of a 8x8x16 slice.
Arguments:
- tokens: bfloat16 [65536, 2048], P(('grp', 'sp', 'tp')), parts along dimension 0, may hold values from -64 to 64
- w_query: bfloat16 [2048, 1024], P(None, 'tp'), may hold values from -0.125 to 0.125
- w_key: bfloat16 [2048, 1024], P(None, 'tp'), may hold values from -0.125 to 0.125
- w_value: bfloat16 [2048, 1024], P(None, 'tp'), may hold values from -0.25 to 0.25
- w_out: bfloat16 [1024, 2048], P('tp'), may hold values from -0.1875 to 0.1875
Outputs:
- mixed: bfloat16 [65536, 2048], P(('grp', 'sp', 'tp')), parts along dimension 0
- log_sums: float32 [16, 65536], P('tp', ('grp', 'sp')), parts along dimension 1
There are 2 independent parts, one for each index of `grp`. A program takes and returns all parts, laid end to end along the dimension named above; an argument that names none is the same for every part. Nothing has to cross between parts.
All inputs are finite; a program needn't handle non-finite values.
Results may differ from a plain program's by a relative error of at most 0.013.
The roundings to bfloat16 on the way count: a program that leaves them out, or rounds other values in their place, can miss the bound.
Values may be sent and summed in bfloat16 or wider, within the bound.
A program may use at most 128 MiB of HBM per device.

v0:
```python
import math

import jax
import jax.numpy as jnp
from jax import lax
from jax.sharding import PartitionSpec as P

HEADS = 16
HEAD_DIM = 64
WINDOW_KEY_STEPS = 128
MIDDLE_DILATION = 4
FAR_DILATION = 16
REACH = 2048


ALIBI_EXP = 16.0


def in_order(pieces, dim):
    shape = list(pieces.shape[1:])
    shape[dim] *= pieces.shape[0]
    return jnp.moveaxis(pieces, 0, dim).reshape(shape)


def sent_to_all(array, axis):
    length = lax.axis_size(axis)
    return lax.all_to_all(
        jnp.broadcast_to(array[None], (length, *array.shape)), axis, 0, 0, tiled=True
    )


def collect(array, axis, dim):
    return in_order(sent_to_all(array, axis), dim)


def shifted(value, axis, steps):
    count = lax.axis_size(axis)
    leading, last = (max(0, -steps), min(count, count - steps))
    return lax.ppermute(value, axis, [(source, source + steps) for source in range(leading, last)])


def in_blocks(array, dim, length):
    before, after = (array.shape[:dim], array.shape[dim + 1 :])
    return jnp.moveaxis(array.reshape(*before, length, -1, *after), dim, 0)


def sum_at_owner(array, axis, dim):
    length = lax.axis_size(axis)
    pieces = lax.all_to_all(in_blocks(array, dim, length), axis, 0, 0, tiled=True)
    return jnp.sum(pieces.astype(jnp.float32), axis=0)


def dilated_attention(queries, key_values, dilation, window_steps, head_slopes, first_position):
    heads, length, depth = queries.shape
    total_rows = key_values.shape[2]
    strided = length // dilation
    block_rows = math.gcd(strided, 128)
    num_blocks = strided // block_rows
    behind = (total_rows - length) // dilation
    grouped = queries.reshape(heads, num_blocks, block_rows, dilation, depth)
    columns = key_values.reshape(2, heads, total_rows // dilation, dilation, depth)
    spans = jnp.stack(
        [
            columns[
                :, :, behind + index * block_rows - window_steps : behind + (index + 1) * block_rows
            ]
            for index in range(num_blocks)
        ],
        axis=2,
    )
    scores = jnp.einsum(
        "hbqre,hbkre->hrbqk", grouped, spans[0], preferred_element_type=jnp.float32
    ) * depth ** (-0.5)
    row_pos = jnp.arange(block_rows, dtype=jnp.int32)[:, None]
    key_pos = jnp.arange(window_steps + block_rows, dtype=jnp.int32)[None, :]
    distance = window_steps + row_pos - key_pos
    inside = (distance >= 0) & (distance <= window_steps)
    block_pos = jnp.arange(num_blocks, dtype=jnp.int32)[None, :, None, None]
    residue = jnp.arange(dilation, dtype=jnp.int32)[:, None, None, None]
    source = (
        first_position
        + (block_pos * block_rows - window_steps + key_pos[None, None]) * dilation
        + residue
    )
    allowed = inside[None, None] & (source >= 0)
    penalty = -head_slopes[:, None, None] * (distance * dilation).astype(jnp.float32)
    scores = jnp.where(allowed[None], scores + penalty[:, None, None], -jnp.inf)
    maxima = jnp.max(scores, axis=-1, keepdims=True)
    weights = jnp.exp(scores - maxima)
    totals = jnp.sum(weights, axis=-1, keepdims=True)
    summed = jnp.einsum(
        "hrbqk,hbkre->hbqre",
        weights.astype(jnp.bfloat16),
        spans[1],
        preferred_element_type=jnp.float32,
    )
    outputs = summed / totals.transpose(0, 2, 3, 1, 4)
    log_part = (maxima + jnp.log(totals))[..., 0]
    outputs = outputs.reshape(heads, length, depth)
    log_part = log_part.transpose(0, 2, 3, 1).reshape(heads, length)
    return (outputs, log_part)


def combine(queries, key_values, head_slopes, first_position):
    heads, length, depth = queries.shape
    window_results = [
        dilated_attention(
            queries, key_values, window_stride, WINDOW_KEY_STEPS, head_slopes, first_position
        )
        for window_stride in (1, MIDDLE_DILATION, FAR_DILATION)
    ]
    stacked = jnp.stack([item[1] for item in window_results])
    log_total = jax.nn.logsumexp(stacked, axis=0)
    hidden = jnp.zeros((heads, length, depth), jnp.float32)
    for item in window_results:
        hidden = hidden + jnp.exp(item[1] - log_total)[..., None] * item[0]
    hidden = hidden.astype(jnp.bfloat16).transpose(1, 0, 2).reshape(length, heads * depth)
    return (hidden, log_total)


def body(tokens, w_query, w_key, w_value, w_out):
    width = w_query.shape[1]
    local_heads = width // HEAD_DIM
    query_heads = w_query.reshape(w_query.shape[0], local_heads, HEAD_DIM)
    key_heads = w_key.reshape(w_key.shape[0], local_heads, HEAD_DIM)
    value_heads = w_value.reshape(w_value.shape[0], local_heads, HEAD_DIM)
    piece = collect(tokens, "tp", 0)
    projected = jnp.stack(
        [
            jnp.einsum(
                "td,dhe->hte", piece, query_heads, preferred_element_type=jnp.float32
            ).astype(jnp.bfloat16),
            jnp.einsum("td,dhe->hte", piece, key_heads, preferred_element_type=jnp.float32).astype(
                jnp.bfloat16
            ),
            jnp.einsum(
                "td,dhe->hte", piece, value_heads, preferred_element_type=jnp.float32
            ).astype(jnp.bfloat16),
        ]
    )
    length = projected.shape[2]
    queries = projected[0]
    key_values = projected[1:]
    hop_count = -(-REACH // length)
    pieces = [key_values]
    carried = key_values
    for distance_dev in range(hop_count):
        carried = shifted(carried, "sp", 1)
        pieces = [carried] + pieces
    window_rows = jnp.concatenate(pieces, axis=2)
    first_position = lax.axis_index("sp") * length
    head_ids = lax.axis_index("tp") * local_heads + jnp.arange(1, local_heads + 1, dtype=jnp.int32)
    head_slopes = jnp.exp2(-ALIBI_EXP * head_ids.astype(jnp.float32) / HEADS)
    hidden, log_total = combine(queries, window_rows, head_slopes, first_position)
    mixed = sum_at_owner(
        jnp.dot(hidden, w_out, preferred_element_type=jnp.float32).astype(jnp.bfloat16), "tp", 0
    ).astype(jnp.bfloat16)
    return (mixed, log_total)


def solution(mesh):
    in_specs = (
        P(("grp", "sp", "tp"), None),
        P(None, "tp"),
        P(None, "tp"),
        P(None, "tp"),
        P("tp", None),
    )
    out_specs = (P(("grp", "sp", "tp"), None), P("tp", ("grp", "sp")))
    return jax.shard_map(body, mesh=mesh, in_specs=in_specs, out_specs=out_specs, check_vma=False)
```

profile of v0, /device:TPU:513, one launch (start us, length us, event | category | flops | bytes accessed | tf_op | source)
XLA Modules:
  0.0 258.0 jit_solution(8653316494520534347)
XLA Ops:
  0.6 3.0 %broadcast_in_dim.39 = bf16[2,256,2048]{2,1,0:T(8,128)(2,1)} broadcast(bf16[256,2048]{1,0:T(8,128)(2,1)} %param.5), dimensions={1,2} | broadcast | bytes 3145728 | tf_op jit(solution)/shard_map/broadcast_in_dim | solution.py:28
  3.6 25.2 %all-to-all-start = ((bf16[2,256,2048]{2,1,0:T(8,128)(2,1)}), bf16[2,256,2048]{2,1,0:T(8,128)(2,1)}, u32[]{:S(2)}, u32[]{:S(2)}) async-start(bf16[2,256,2048]{2,1,0:T(8,128)(2,1)} %broadcast_in_dim.39), calls=%async_computation | async-start | bytes 4194304 | tf_op jit(solution)/shard_map/all_to_all | solution.py:27
  28.8 4.0 %copy.93 = bf16[2048,512]{0,1:T(8,128)(2,1)} copy(bf16[2048,512]{1,0:T(8,128)(2,1)} %param.8) | data formatting | bytes 4194304 | tf_op args[3]
  32.8 4.0 %copy.92 = bf16[2048,512]{0,1:T(8,128)(2,1)} copy(bf16[2048,512]{1,0:T(8,128)(2,1)} %param.7) | data formatting | bytes 4194304 | tf_op args[2]
  36.7 3.7 %fusion.32 = bf16[1,8,512,64]{2,3,1,0:T(8,128)(2,1)S(1)} fusion(bf16[2048,8,64]{0,2,1:T(8,128)(2,1)} %bitcast.138, bf16[512,2048,1]{1,0,2:T(8,128)(2,1)} %bitcast.2), kind=kOutput, calls=%fused_computation.37 | convolution fusion | flops 1074003968 | bytes 4718592 | tf_op jit(solution)/shard_map/td,dhe->hte/dot_general | solution.py:136
  40.4 3.1 %fusion.31 = bf16[1,8,512,64]{2,3,1,0:T(8,128)(2,1)S(1)} fusion(bf16[2048,8,64]{0,2,1:T(8,128)(2,1)S(1)} %bitcast.137, bf16[512,2048,1]{1,0,2:T(8,128)(2,1)} %bitcast.2), kind=kOutput, calls=%fused_computation.36 | convolution fusion | flops 1074003968 | bytes 4718592 | tf_op jit(solution)/shard_map/td,dhe->hte/dot_general | solution.py:133
  43.6 2.3 collective-permute-start
  45.9 4.0 %copy.91 = bf16[2048,512]{0,1:T(8,128)(2,1)} copy(bf16[2048,512]{1,0:T(8,128)(2,1)} %param.6) | data formatting | bytes 4194304 | tf_op args[1]
  49.9 17.8 %collective-permute-done = bf16[2,8,512,64]{2,3,1,0:T(8,128)(2,1)} collective-permute-done((bf16[2,8,512,64]{2,3,1,0:T(8,128)(2,1)S(1)}, bf16[2,8,512,64]{2,3,1,0:T(8,128)(2,1)}, u32[]{:S(2)}, u32[]{:S(2)}) %collective-permute-start) | collective-permute-done | bytes 1048608 | tf_op jit(solution)/shard_map/ppermute | solution.py:39
  67.7 5.2 %collective-permute-start.1 = (bf16[2,8,512,64]{2,3,1,0:T(8,128)(2,1)}, bf16[2,8,512,64]{2,3,1,0:T(8,128)(2,1)}, u32[]{:S(2)}, u32[]{:S(2)}) collective-permute-start(bf16[2,8,512,64]{2,3,1,0:T(8,128)(2,1)} %collective-permute-done), channel_id=1, source_target_pairs={{0,2},{2,4},{4,6},{6,8},{8,10},{10,12},{12,14},{14,16},{16,18},{18... | collective-permute-start | bytes 3145736 | tf_op jit(solution)/shard_map/ppermute | solution.py:39
  73.0 3.5 %convolution_convert_fusion.3 = bf16[8,64,512]{2,1,0:T(8,128)(2,1)S(1)} fusion(bf16[2048,8,64]{0,2,1:T(8,128)(2,1)} %bitcast.136, bf16[512,2048,1]{1,0,2:T(8,128)(2,1)} %bitcast.2), kind=kOutput, calls=%fused_computation.35 | convolution fusion | flops 1074003968 | bytes 4718592 | tf_op jit(solution)/shard_map/td,dhe->hte/dot_general | solution.py:130
  76.5 17.6 %collective-permute-done.1 = bf16[2,8,512,64]{2,3,1,0:T(8,128)(2,1)} collective-permute-done((bf16[2,8,512,64]{2,3,1,0:T(8,128)(2,1)}, bf16[2,8,512,64]{2,3,1,0:T(8,128)(2,1)}, u32[]{:S(2)}, u32[]{:S(2)}) %collective-permute-start.1) | collective-permute-done | bytes 1048608 | tf_op jit(solution)/shard_map/ppermute | solution.py:39
  94.1 5.1 %collective-permute-start.2 = (bf16[2,8,512,64]{2,3,1,0:T(8,128)(2,1)}, bf16[2,8,512,64]{2,3,1,0:T(8,128)(2,1)}, u32[]{:S(2)}, u32[]{:S(2)}) collective-permute-start(bf16[2,8,512,64]{2,3,1,0:T(8,128)(2,1)} %collective-permute-done.1), channel_id=1, source_target_pairs={{0,2},{2,4},{4,6},{6,8},{8,10},{10,12},{12,14},{14,16},{16,18},{18... | collective-permute-start | bytes 3145736 | tf_op jit(solution)/shard_map/ppermute | solution.py:39
  99.2 1.3 copy.101
  100.5 1.7 copy.96
  102.6 16.9 %collective-permute-done.2 = bf16[2,8,512,64]{2,3,1,0:T(8,128)(2,1)} collective-permute-done((bf16[2,8,512,64]{2,3,1,0:T(8,128)(2,1)}, bf16[2,8,512,64]{2,3,1,0:T(8,128)(2,1)}, u32[]{:S(2)}, u32[]{:S(2)}) %collective-permute-start.2) | collective-permute-done | bytes 1048608 | tf_op jit(solution)/shard_map/ppermute | solution.py:39
  119.6 4.4 %collective-permute-start.3 = (bf16[2,8,512,64]{2,3,1,0:T(8,128)(2,1)}, bf16[2,8,512,64]{2,3,1,0:T(8,128)(2,1)S(1)}, u32[]{:S(2)}, u32[]{:S(2)}) collective-permute-start(bf16[2,8,512,64]{2,3,1,0:T(8,128)(2,1)} %collective-permute-done.2), channel_id=1, source_target_pairs={{0,2},{2,4},{4,6},{6,8},{8,10},{10,12},{12,14},{14,16},{16,18},{18... | collective-permute-start | bytes 3145736 | tf_op jit(solution)/shard_map/ppermute | solution.py:39
  126.2 18.0 %collective-permute-done.3 = bf16[2,8,512,64]{2,3,1,0:T(8,128)(2,1)S(1)} collective-permute-done((bf16[2,8,512,64]{2,3,1,0:T(8,128)(2,1)}, bf16[2,8,512,64]{2,3,1,0:T(8,128)(2,1)S(1)}, u32[]{:S(2)}, u32[]{:S(2)}) %collective-permute-start.3) | collective-permute-done | bytes 1048608 | tf_op jit(solution)/shard_map/ppermute | solution.py:39
  144.3 1.3 constant_dynamic-update-slice_fusion.3
  145.6 1.3 constant_dynamic-update-slice_fusion.2
  146.9 1.3 constant_dynamic-update-slice_fusion.1
  148.3 2.4 copy-done.1
  150.6 2.8 %fusion.74 = (bf16[1,8,2560,64]{2,3,1,0:T(8,128)(2,1)}, bf16[1,8,2560,64]{2,3,1,0:T(8,128)(2,1)}) fusion(bf16[2,8,2560,64]{2,3,1,0:T(8,128)(2,1)S(1)} %constant_dynamic-update-slice_fusion), kind=kLoop, calls=%fused_computation.110 | loop fusion | bytes 10485760 | tf_op jit(solution)/shard_map/slice | solution.py:94
  153.4 12.2 %copy.97 = bf16[2,8,2560,64]{3,1,2,0:T(8,128)(2,1)} copy(bf16[2,8,2560,64]{2,3,1,0:T(8,128)(2,1)} %copy-done.1) | data formatting | bytes 10485760 | tf_op jit(solution)/shard_map/concatenate | solution.py:150
  165.6 6.0 %copy.102 = bf16[1,8,2560,64]{3,2,1,0:T(8,128)(2,1)} copy(bf16[1,8,2560,64]{2,3,1,0:T(8,128)(2,1)} %get-tuple-element.15) | data formatting | bytes 5242880 | tf_op jit(solution)/shard_map/slice | solution.py:72
  171.5 6.3 %fusion.12 = (f32[8,16,32]{2,1,0:T(8,128)S(1)}, f32[8,16,32,160]{3,2,1,0:T(8,128)S(1)}) fusion(f32[8,32,160]{2,1,0:T(8,128)} %broadcast_multiply_fusion.2, pred[16,32,160]{2,1,0:T(8,128)(4,1)S(1)} %broadcast_and_fusion, bf16[8,160,16,64]{3,2,1,0:T(8,128)(2,1)} %bitcast.130, bf16[8,32,16,64]{3,2,1,0:T(8,128)(2,1)} %bitcast.140), kind=kOutput, calls=%fused_computation.19 | convolution fusion | flops 86503424 | bytes 6029312 | tf_op jit(solution)/shard_map/hbqre,hbkre->hrbqk/dot_general | solution.py:71
  177.8 2.0 copy-done.10
  179.8 1.7 fusion.9
  184.6 6.0 %copy.116 = bf16[1,8,2560,64]{3,2,1,0:T(8,128)(2,1)} copy(bf16[1,8,2560,64]{2,3,1,0:T(8,128)(2,1)} %get-tuple-element.14) | data formatting | bytes 5242880 | tf_op jit(solution)/shard_map/slice | solution.py:94
  190.6 5.4 %bitcast_divide_fusion = f32[8,1,32,16,64]{4,2,3,0,1:T(8,128)S(1)} fusion(f32[8,32,16]{1,2,0:T(8,128)} %bitcast.142, bf16[8,160,16,64]{3,2,1,0:T(8,128)(2,1)} %bitcast.129, f32[8,16,32,160]{3,2,1,0:T(8,128)} %copy-done.10, f32[8,16,32]{2,1,0:T(8,128)} %copy-done.20, f32[8,32,160]{2,1,0:T(8,128)} %broadcast_multiply_fusion.2, ...), kind=kOutput, calls=%fused_computation.21 | convolution fusion | flops 87425024 | bytes 6569984 | tf_op jit(solution)/shard_map/hrbqk,hbkre->hbqre/dot_general | solution.py:91
  195.9 2.5 copy.118
  198.4 3.1 %copy.119 = f32[8,512,64]{1,2,0:T(8,128)} copy(f32[8,512,64]{2,1,0:T(8,128)} %bitcast.128) | data formatting | bytes 2097152 | tf_op jit(solution)/shard_map/reshape | solution.py:99
  201.6 4.9 %fusion.73 = (bf16[1,8,256,4,64]{4,1,3,2,0:T(8,128)(2,1)}, bf16[1,8,256,4,64]{4,1,3,2,0:T(8,128)(2,1)}) fusion(bf16[2,8,640,4,64]{4,1,3,2,0:T(8,128)(2,1)} %bitcast.126), kind=kLoop, calls=%fused_computation.109 | loop fusion | bytes 4194304 | tf_op jit(solution)/shard_map/slice | solution.py:94
  206.5 3.6 %copy.120 = bf16[1,8,256,4,64]{2,4,3,1,0:T(8,128)(2,1)} copy(bf16[1,8,256,4,64]{4,1,3,2,0:T(8,128)(2,1)} %get-tuple-element.9) | data formatting | bytes 2097152
  210.1 3.6 %copy.121 = bf16[1,8,256,4,64]{2,4,3,1,0:T(8,128)(2,1)} copy(bf16[1,8,256,4,64]{4,1,3,2,0:T(8,128)(2,1)} %get-tuple-element.8) | data formatting | bytes 2097152
  213.6 1.7 slice_bitcast_fusion.5
  216.8 1.4 fusion.10
  218.3 1.6 fusion.11
  219.9 3.6 %fusion.5 = (f32[8,4,128]{2,1,0:T(4,128)S(1)}, f32[8,4,128]{2,1,0:T(4,128)S(1)}) fusion(f32[8,4,128,256]{3,2,1,0:T(8,128)S(1)} %get-tuple-element.31, f32[8,4,128]{2,1,0:T(4,128)S(1)} %get-tuple-element.30, f32[8,128,256]{2,1,0:T(8,128)S(1)} %copy-done.3, pred[4,128,256]{2,1,0:T(8,128)(4,1)S(1)} %get-tuple-element.18, ...), kind=kLoop, calls=%fused_computation.11 | loop fusion | flops 10477568 | bytes 10813440 | tf_op jit(solution)/shard_map/reduce_sum | solution.py:90
  223.5 2.6 fusion.41
  226.1 4.2 %copy.114 = f32[8,1,128,4,64]{4,0,3,2,1:T(8,128)} copy(f32[8,1,128,4,64]{2,4,3,0,1:T(8,128)} %fusion.41) | data formatting | bytes 2097152 | tf_op jit(solution)/shard_map/div | solution.py:97
  230.3 3.2 %copy.115 = f32[8,512,64]{1,2,0:T(8,128)} copy(f32[8,512,64]{2,0,1:T(8,128)} %bitcast.127) | data formatting | bytes 2097152 | tf_op jit(solution)/shard_map/reshape | solution.py:99
  233.5 3.9 %divide_bitcast_fusion = f32[8,4,128,1,64]{2,4,1,0,3:T(8,128)S(1)} fusion(f32[8,4,128,256]{3,2,1,0:T(8,128)} %copy-done.2, f32[8,4,128]{2,1,0:T(4,128)S(1)} %get-tuple-element.30, f32[8,128,256]{2,1,0:T(8,128)S(1)} %copy-done.4, pred[4,128,256]{2,1,0:T(8,128)(4,1)S(1)} %get-tuple-element.18, bf16[8,4,256,64]{2,3,0,1:T(8,128)(2,1)} %get-tuple-element.16, ...), kind=kOutput, calls=%fused_computation.50 | convolution fusion | flops 139722752 | bytes 7503872 | tf_op jit(solution)/shard_map/hrbqk,hbkre->hbqre/dot_general | solution.py:91
  237.5 1.7 copy.111
  239.1 2.6 %reshape.599 = f32[8,512,64]{1,2,0:T(8,128)} reshape(f32[8,4,128,1,64]{2,1,4,0,3:T(4,128)} %copy.111) | data formatting | bytes 2097152 | tf_op jit(solution)/shard_map/reshape | solution.py:99
  242.3 2.0 add_convert_fusion
  245.5 9.1 %all_to_all.10 = bf16[2,256,2048]{2,1,0:T(8,128)(2,1)} all-to-all(bf16[2,256,2048]{2,1,0:T(8,128)(2,1)S(1)} %bitcast.139), channel_id=1, replica_groups=mesh['grp'=2,'sp'=64,'tp'=2] {'tp'}, dimensions={0} | all-to-all | bytes 4194304 | tf_op jit(solution)/shard_map/all_to_all | solution.py:49
  254.7 3.3 %reduce_sum.52 = bf16[256,2048]{1,0:T(8,128)(2,1)} reduce(bf16[2,256,2048]{2,1,0:T(8,128)(2,1)} %all_to_all.10, bf16[]{:T(256)} %constant.29.clone.1), dimensions={0}, to_apply=%region_7.8 | reduce | flops 524288 | bytes 3145730 | tf_op jit(solution)/shard_map/reduce_sum | solution.py:50
  (84 shorter events, 9.2 us)
Async XLA Ops:
  0.6 243.6 %copy-start = (bf16[512,2048]{1,0:T(8,128)(2,1)S(1)}, bf16[512,2048]{1,0:T(8,128)(2,1)}, u32[]{:S(2)}) copy-start(bf16[512,2048]{1,0:T(8,128)(2,1)} %param.9) | copy-start | bytes 6291460
  3.6 33.1 %all-to-all-start = ((bf16[2,256,2048]{2,1,0:T(8,128)(2,1)}), bf16[2,256,2048]{2,1,0:T(8,128)(2,1)}, u32[]{:S(2)}, u32[]{:S(2)}) async-start(bf16[2,256,2048]{2,1,0:T(8,128)(2,1)} %broadcast_in_dim.39), calls=%async_computation | async-start | bytes 4194304 | tf_op jit(solution)/shard_map/all_to_all | solution.py:27
  36.7 3.7 %copy-start.11 = (bf16[2048,512]{0,1:T(8,128)(2,1)S(1)}, bf16[2048,512]{0,1:T(8,128)(2,1)}, u32[]{:S(2)}) copy-start(bf16[2048,512]{0,1:T(8,128)(2,1)} %copy.92) | copy-start | bytes 6291460
  40.4 3.2 %copy-start.12 = (bf16[1,8,512,64]{2,3,1,0:T(8,128)(2,1)}, bf16[1,8,512,64]{2,3,1,0:T(8,128)(2,1)S(1)}, u32[]{:S(2)}) copy-start(bf16[1,8,512,64]{2,3,1,0:T(8,128)(2,1)S(1)} %fusion.32) | copy-start | bytes 1572868
  43.5 2.4 copy-start.14
  43.6 24.1 %collective-permute-start = (bf16[2,8,512,64]{2,3,1,0:T(8,128)(2,1)S(1)}, bf16[2,8,512,64]{2,3,1,0:T(8,128)(2,1)}, u32[]{:S(2)}, u32[]{:S(2)}) collective-permute-start(bf16[2,8,512,64]{2,3,1,0:T(8,128)(2,1)S(1)} %pad_maximum_fusion.1), channel_id=1, source_target_pairs={{0,2},{2,4},{4,6},{6,8},{8,10},{10,12},{12,14},{14,16},{16,18},{18... | collective-permute-start | bytes 3145736 | tf_op jit(solution)/shard_map/ppermute | solution.py:39
  67.7 26.4 %collective-permute-start.1 = (bf16[2,8,512,64]{2,3,1,0:T(8,128)(2,1)}, bf16[2,8,512,64]{2,3,1,0:T(8,128)(2,1)}, u32[]{:S(2)}, u32[]{:S(2)}) collective-permute-start(bf16[2,8,512,64]{2,3,1,0:T(8,128)(2,1)} %collective-permute-done), channel_id=1, source_target_pairs={{0,2},{2,4},{4,6},{6,8},{8,10},{10,12},{12,14},{14,16},{16,18},{18... | collective-permute-start | bytes 3145736 | tf_op jit(solution)/shard_map/ppermute | solution.py:39
  76.5 48.5 %copy-start.5 = (bf16[8,64,512]{2,1,0:T(8,128)(2,1)}, bf16[8,64,512]{2,1,0:T(8,128)(2,1)S(1)}, u32[]{:S(2)}) copy-start(bf16[8,64,512]{2,1,0:T(8,128)(2,1)S(1)} %convolution_convert_fusion.3) | copy-start | bytes 1572868
  94.1 25.5 %collective-permute-start.2 = (bf16[2,8,512,64]{2,3,1,0:T(8,128)(2,1)}, bf16[2,8,512,64]{2,3,1,0:T(8,128)(2,1)}, u32[]{:S(2)}, u32[]{:S(2)}) collective-permute-start(bf16[2,8,512,64]{2,3,1,0:T(8,128)(2,1)} %collective-permute-done.1), channel_id=1, source_target_pairs={{0,2},{2,4},{4,6},{6,8},{8,10},{10,12},{12,14},{14,16},{16,18},{18... | collective-permute-start | bytes 3145736 | tf_op jit(solution)/shard_map/ppermute | solution.py:39
  102.6 75.2 %copy-start.18 = (pred[16,32,160]{2,1,0:T(8,128)(4,1)}, pred[16,32,160]{2,1,0:T(8,128)(4,1)S(1)}, u32[]{:S(2)}) copy-start(pred[16,32,160]{2,1,0:T(8,128)(4,1)S(1)} %broadcast_and_fusion) | copy-start | bytes 245764
  119.6 24.6 %collective-permute-start.3 = (bf16[2,8,512,64]{2,3,1,0:T(8,128)(2,1)}, bf16[2,8,512,64]{2,3,1,0:T(8,128)(2,1)S(1)}, u32[]{:S(2)}, u32[]{:S(2)}) collective-permute-start(bf16[2,8,512,64]{2,3,1,0:T(8,128)(2,1)} %collective-permute-done.2), channel_id=1, source_target_pairs={{0,2},{2,4},{4,6},{6,8},{8,10},{10,12},{12,14},{14,16},{16,18},{18... | collective-permute-start | bytes 3145736 | tf_op jit(solution)/shard_map/ppermute | solution.py:39
  126.2 22.0 %copy-start.13 = (bf16[1,8,512,64]{2,3,1,0:T(8,128)(2,1)S(1)}, bf16[1,8,512,64]{2,3,1,0:T(8,128)(2,1)}, u32[]{:S(2)}) copy-start(bf16[1,8,512,64]{2,3,1,0:T(8,128)(2,1)} %copy-done.12) | copy-start | bytes 1572868
  126.2 22.0 %copy-start.15 = (bf16[1,8,512,64]{2,3,1,0:T(8,128)(2,1)S(1)}, bf16[1,8,512,64]{2,3,1,0:T(8,128)(2,1)}, u32[]{:S(2)}) copy-start(bf16[1,8,512,64]{2,3,1,0:T(8,128)(2,1)} %copy-done.14) | copy-start | bytes 1572868
  148.3 2.4 copy-start.1
  171.5 8.3 %copy-start.17 = (f32[8,32,160]{2,1,0:T(8,128)S(1)}, f32[8,32,160]{2,1,0:T(8,128)}, u32[]{:S(2)}) copy-start(f32[8,32,160]{2,1,0:T(8,128)} %broadcast_multiply_fusion.2) | copy-start | bytes 491524
  177.8 2.0 copy-start.10
  177.8 3.7 %copy-start.20 = (f32[8,16,32]{2,1,0:T(8,128)}, f32[8,16,32]{2,1,0:T(8,128)S(1)}, u32[]{:S(2)}) copy-start(f32[8,16,32]{2,1,0:T(8,128)S(1)} %get-tuple-element.26) | copy-start | bytes 49156
  181.5 0.6 copy-start.21
  184.6 6.0 %copy-start.19 = (pred[16,32,160]{2,1,0:T(8,128)(4,1)S(1)}, pred[16,32,160]{2,1,0:T(8,128)(4,1)}, u32[]{:S(2)}) copy-start(pred[16,32,160]{2,1,0:T(8,128)(4,1)} %copy-done.18) | copy-start | bytes 245764
  215.3 1.4 copy-start.3
  215.3 1.4 copy-start.6
  216.7 1.4 copy-start.8
  216.7 1.5 copy-start.9
  218.2 5.4 %copy-start.2 = (f32[8,4,128,256]{3,2,1,0:T(8,128)}, f32[8,4,128,256]{3,2,1,0:T(8,128)S(1)}, u32[]{:S(2)}) copy-start(f32[8,4,128,256]{3,2,1,0:T(8,128)S(1)} %get-tuple-element.31) | copy-start | bytes 12582916
  219.8 3.7 %copy-start.16 = (bf16[1,8,256,4,64]{2,4,3,1,0:T(8,128)(2,1)S(1)}, bf16[1,8,256,4,64]{2,4,3,1,0:T(8,128)(2,1)}, u32[]{:S(2)}) copy-start(bf16[1,8,256,4,64]{2,4,3,1,0:T(8,128)(2,1)} %copy.121) | copy-start | bytes 3145732
  226.1 7.4 %copy-start.4 = (f32[8,128,256]{2,1,0:T(8,128)S(1)}, f32[8,128,256]{2,1,0:T(8,128)}, u32[]{:S(2)}) copy-start(f32[8,128,256]{2,1,0:T(8,128)} %get-tuple-element.22) | copy-start | bytes 3145732
  237.4 4.7 %copy-start.22 = (f32[1,8,512]{2,1,0:T(8,128)S(1)}, f32[1,8,512]{2,1,0:T(8,128)}, u32[]{:S(2)}) copy-start(f32[1,8,512]{2,1,0:T(8,128)} %stack_reshape.12) | copy-start | bytes 49156
  237.4 4.8 %copy-start.7 = (f32[8,512,64]{1,2,0:T(8,128)S(1)}, f32[8,512,64]{1,2,0:T(8,128)}, u32[]{:S(2)}) copy-start(f32[8,512,64]{1,2,0:T(8,128)} %copy.119) | copy-start | bytes 3145732
  242.2 3.3 %copy-start.23 = (f32[8,512]{1,0:T(8,128)}, f32[8,512]{1,0:T(8,128)S(1)}, u32[]{:S(2)}) copy-start(f32[8,512]{1,0:T(8,128)S(1)} %get-tuple-element.7) | copy-start | bytes 49156
where the time goes:
time: 259 us; the launch traced here: 258 us
  local copies, waits for them, and re-layouts  88.2 us (34%)
  waiting for transfers between devices  70.3 us (27%)
  starting transfers between devices  42.2 us (16%)
  matrix products  32.6 us (13%)
  other arithmetic  14.5 us (6%)
  blocking collectives  9.14 us (4%)
    ppermute x4, waiting for transfers between devices, shifted(): lax.ppermute(value, axis, [(source, source + steps) for source in range(l...  70.3 us
    unnamed x57, local copies, waits for them, and re-layouts  28.1 us
    all_to_all x1, starting transfers between devices, sent_to_all(): lax.all_to_all(jnp.broadcast_to(array[None], (length, *array.shape)), axi...  25.2 us
    ppermute x4, starting transfers between devices, shifted(): lax.ppermute(value, axis, [(source, source + steps) for source in range(l...  17 us
    slice x3, local copies, waits for them, and re-layouts, dilated_attention(): spans[1]  13.7 us
    concatenate x1, local copies, waits for them, and re-layouts, body(): window_rows = jnp.concatenate(pieces, axis=2)  12.2 us
    dot_general x3, matrix products, dilated_attention(): jnp.einsum('hrbqk,hbkre->hbqre', weights.astype(jnp.bfloat16), spans[1],...  11.9 us
    dot_general x3, matrix products, dilated_attention(): jnp.einsum('hbqre,hbkre->hrbqk', grouped, spans[0], preferred_element_typ...  9.22 us
  transfers between devices with their start and end apart: 5, of which 4 were waited for; matrix products, arithmetic and copies ran while one was open for 8% of the time, Pallas kernels for 0%

commit v1 on v0

v1 whole, which is shorter than its diff:
```python
import functools

import jax
import jax.numpy as jnp
from jax import lax
from jax.experimental import pallas as pl
from jax.experimental.pallas import tpu as pltpu
from jax.sharding import PartitionSpec as P

HEADS = 16
HEAD_DIM = 64
STEPS = 128
REACH = 2048
ALIBI_EXP = 16.0
STRIDE = 16
LANES = 128
MASKED = -1e30
MESH = pl.DeviceIdType.MESH
F32 = jnp.float32
BF16 = jnp.bfloat16


def iota(shape, dim):
    return lax.broadcasted_iota(jnp.int32, shape, dim)


def permuted(m):
    return (m // LANES) * LANES + (m % 8) * STRIDE + (m % LANES) // 8


def kernel(
    rows_sp, tok, wq, wk, wv, wo, mixed, logs,
    x_in, x_perm, q_w, k_w, v_w, o_w, k_tmp, send_kv, send_q, kv, kv1, q_pk, q_near, q_far, k_far, k_far1,
    bias, far_r, far_m, mid_r, mid_m, o_send, o_recv, l_send, l_recv, l_nat, hid, part, other,
    load_sem, tok_sem, kv_s, kv_r, q_s, q_r, halo_s, halo_r, o_s, o_r, l_s, l_r, part_s, part_r, in_sem,
):
    half, depth = tok.shape
    block = 2 * half
    group = q_w.shape[1] // HEAD_DIM
    halo = REACH // block
    far_rows = block // STRIDE
    sp, tp = lax.axis_index("sp"), lax.axis_index("tp")
    x = lax.rem(sp, group)
    base = sp - x
    y = sp // group
    up = rows_sp - 1

    def peer(d):
        return {"sp": base + d, "tp": tp}

    partner = {"tp": 1 - tp}

    mine = pl.multiple_of(tp * half, half)
    loads = [
        pltpu.make_async_copy(tok, x_in.at[pl.ds(mine, half)], load_sem.at[0]),
        pltpu.make_async_copy(wk, k_w, load_sem.at[1]),
        pltpu.make_async_copy(wv, v_w, load_sem.at[2]),
        pltpu.make_async_copy(wq, q_w, load_sem.at[3]),
        pltpu.make_async_copy(wo, o_w, load_sem.at[4]),
    ]
    for c in loads:
        c.start()

    barrier = pltpu.get_barrier_semaphore()
    pl.semaphore_signal(barrier, inc=1, device_id=partner, device_id_type=MESH)
    for d in range(group):
        @pl.when(d < x)
        def _():
            pl.semaphore_signal(barrier, inc=1, device_id=peer(d), device_id_type=MESH)

    @pl.when(y > 0)
    def _():
        pl.semaphore_signal(barrier, inc=1, device_id={"sp": sp - group, "tp": tp}, device_id_type=MESH)

    head = (tp * group + x + 1).astype(F32)
    slope = jnp.exp2(jnp.full((LANES, 2 * LANES), -ALIBI_EXP / HEADS, F32) * head)
    row, col = iota((LANES, 2 * LANES), 0), iota((LANES, 2 * LANES), 1)
    near_d = STEPS + permuted(row) - (col // LANES) * LANES - permuted(col % LANES)
    mid_d = STEPS + 4 * (row % 32) + row // 32 - ((col % 64) // 32) * LANES - 4 * (col % 32) - col // 64
    far_d = STEPS + row - col
    before = (col < LANES, (col % 64) < 32, col < LANES)
    for w, (dist, stride) in enumerate(((near_d, 1), (mid_d, 4), (far_d, 16))):
        plain = jnp.where((dist >= 0) & (dist <= STEPS), -slope * (dist * stride).astype(F32), MASKED)
        bias[2 * w] = plain
        bias[2 * w + 1] = jnp.where(before[w] & (y == 0), MASKED, plain)

    low = iota((half, LANES), 1) < HEAD_DIM

    @pl.when(y == 0)
    def _():
        kv[pl.ds(0, REACH), :] = jnp.zeros((REACH, LANES), BF16)

    pl.semaphore_wait(barrier, group - x + jnp.where(y < up, 1, 0))
    for d in range(group):
        @pl.when(d > x)
        def _():
            pl.semaphore_signal(in_sem.at[x], inc=1, device_id=peer(d), device_id_type=MESH)

    loads[0].wait()
    tok_copy = pltpu.make_async_remote_copy(
        src_ref=x_in.at[pl.ds(mine, half)], dst_ref=x_in.at[pl.ds(mine, half)],
        send_sem=tok_sem.at[0], recv_sem=tok_sem.at[1], device_id=partner, device_id_type=MESH)
    tok_copy.start()
    pm, pt = iota((half, half), 0), iota((half, half), 1)
    perm = jnp.where(permuted(pm) == pt, 1.0, 0.0).astype(BF16)
    back = jnp.where(permuted(pt) == pm, 1.0, 0.0).astype(BF16)

    def permute(first):
        x_perm[pl.ds(first, half), :] = jnp.dot(perm, x_in[pl.ds(first, half), :], preferred_element_type=F32).astype(BF16)

    permute(mine)
    other_half = pl.multiple_of((1 - tp) * half, half)
    their_copy = pltpu.make_async_remote_copy(
        src_ref=x_in.at[pl.ds(mine, half)], dst_ref=x_in.at[pl.ds(other_half, half)],
        send_sem=tok_sem.at[0], recv_sem=tok_sem.at[1], device_id=partner, device_id_type=MESH)
    their_copy.wait_recv()
    permute(other_half)

    def kv_copy(d, source):
        return pltpu.make_async_remote_copy(
            src_ref=send_kv.at[d], dst_ref=kv.at[pl.ds(pl.multiple_of(REACH + source * block, block), block)],
            send_sem=kv_s.at[d], recv_sem=kv_r.at[source], device_id=peer(d), device_id_type=MESH)

    def q_copy(d, source):
        return pltpu.make_async_remote_copy(
            src_ref=send_q.at[d], dst_ref=q_pk.at[source],
            send_sem=q_s.at[d], recv_sem=q_r.at[source], device_id=peer(d), device_id_type=MESH)

    own_kv = pltpu.make_async_copy(send_kv.at[x], kv.at[pl.ds(pl.multiple_of(REACH + x * block, block), block)], kv_s.at[x])
    own_q = pltpu.make_async_copy(send_q.at[x], q_pk.at[x], q_s.at[x])

    for c in loads[1:4]:
        c.wait()
    wide = 2 * LANES
    heads_at_once = wide // HEAD_DIM
    low_block = iota((block, LANES), 1) < HEAD_DIM
    order = (4, 3, 5, 2, 6, 1, 7)
    for g in reversed(range(group // heads_at_once)):
        cols = slice(g * wide, (g + 1) * wide)
        k_tmp[...] = jnp.dot(x_perm[...], k_w[:, cols], preferred_element_type=F32)
        v_all = jnp.dot(x_perm[...], v_w[:, cols], preferred_element_type=F32)
        for p in range(2):
            k_p, v_p = k_tmp[:, p * LANES:(p + 1) * LANES], v_all[:, p * LANES:(p + 1) * LANES]
            d = g * heads_at_once + 2 * p
            send_kv[d] = jnp.where(low_block, k_p, pltpu.roll(v_p, HEAD_DIM, 1)).astype(BF16)
            send_kv[d + 1] = jnp.where(low_block, pltpu.roll(k_p, HEAD_DIM, 1), v_p).astype(BF16)
        q_all = jnp.dot(x_perm[...], q_w[:, cols], preferred_element_type=F32) * HEAD_DIM ** -0.5
        for p in range(2):
            q_a, q_b = q_all[:half, p * LANES:(p + 1) * LANES], q_all[half:, p * LANES:(p + 1) * LANES]
            d = g * heads_at_once + 2 * p
            send_q[d] = jnp.where(low, q_a, pltpu.roll(q_b, HEAD_DIM, 1)).astype(BF16)
            send_q[d + 1] = jnp.where(low, pltpu.roll(q_a, HEAD_DIM, 1), q_b).astype(BF16)
        for step in order:
            d = lax.rem(x + step, group)

            @pl.when((d // heads_at_once == g) & (d > 0))
            def _():
                @pl.when(d < x)
                def _():
                    pl.semaphore_wait(in_sem.at[d], 1)

                kv_copy(d, x).start()
                q_copy(d, x).start()

        @pl.when(x // heads_at_once == g)
        def _():
            own_kv.start()
            own_q.start()

    @pl.when(x > 0)
    def _():
        pl.semaphore_wait(in_sem.at[0], 1)
        kv_copy(0, x).start()
        q_copy(0, x).start()

    lane_low = iota((half, LANES), 1) < HEAD_DIM

    def to_far(ref, values, slot, part_index):
        for r in range(STRIDE):
            pair = jnp.concatenate([values[8 * r:8 * r + 8], values[LANES + 8 * r:LANES + 8 * r + 8]], axis=0)
            ref[r, pl.ds(pl.multiple_of(far_rows * slot + 16 * part_index, 16), 16), :] = pair.astype(BF16)

    def take_keys(slot):
        for h in range(2):
            first = pl.multiple_of(slot * block + h * half, half)
            values = kv[pl.ds(first, half), :].astype(F32)
            with_ones = jnp.where(lane_low, 1.0, values)
            kv1[pl.ds(first, half), :] = with_ones.astype(BF16)
            to_far(k_far, values, slot, h)
            to_far(k_far1, with_ones, slot, h)

    def take_queries(b):
        values = q_pk[b].astype(F32)
        for h in range(2):
            part_q = jnp.where(lane_low, values if h == 0 else pltpu.roll(values, HEAD_DIM, 1), 0.0)
            q_near[pl.ds(pl.multiple_of(b * block + h * half, half), half), :] = part_q.astype(BF16)
            to_far(q_far, part_q, b, h)

    def halo_copy(b):
        return pltpu.make_async_remote_copy(
            src_ref=kv.at[pl.ds(pl.multiple_of(REACH + b * block, block), block)],
            dst_ref=kv.at[pl.ds(pl.multiple_of((b - (group - halo)) * block, block), block)],
            send_sem=halo_s.at[b - (group - halo)], recv_sem=halo_r.at[b - (group - halo)],
            device_id={"sp": sp + group, "tp": tp}, device_id_type=MESH)

    def pass_on(b):
        @pl.when((b >= group - halo) & (y < up))
        def _():
            halo_copy(b).start()

    own_kv.wait()
    own_q.wait()
    pass_on(x)
    take_keys(x + halo)
    take_queries(x)

    def arrive(i, carry):
        b = lax.rem(x + i, group)
        kv_copy(b, b).wait_recv()
        pass_on(b)
        take_keys(b + halo)
        q_copy(b, b).wait_recv()
        take_queries(b)
        return carry

    lax.fori_loop(1, group, arrive, 0)

    def take_halo(i, carry):
        @pl.when(y > 0)
        def _():
            halo_copy(i + group - halo).wait_recv()

        take_keys(i)
        return carry

    lax.fori_loop(0, halo, take_halo, 0)

    def scores(q, keys, which):
        s = lax.dot_general(q, keys, (((1,), (1,)), ((), ())), preferred_element_type=F32) + bias[which]
        m = jnp.max(s, axis=1, keepdims=True)
        return jnp.exp(s - m).astype(BF16), m

    first_row = jnp.where(y == 0, 1, 0)
    eights = [(c, pl.ds(8 * c, 8)) for c in range(LANES // 8)]

    def far_step(i, carry):
        for rr in range(2):
            r = 2 * i + rr
            for qb in range(group * far_rows // LANES):
                keys = pl.ds(qb * LANES, 2 * LANES)
                w, m = scores(q_far[r, pl.ds(qb * LANES, LANES), :], k_far[r, keys, :], 4 + (1 if qb == 0 else 0))
                res = jnp.dot(w, k_far1[r, keys, :], preferred_element_type=F32)
                m_all = jnp.broadcast_to(m, (LANES, LANES))
                for c in range(LANES // 8):
                    dst = (qb * (LANES // far_rows) + c // 4) * block + (c % 4) * LANES
                    at = pl.ds(pl.multiple_of(dst + 8 * r, 8), 8)
                    far_r[at, :] = res[8 * c:8 * c + 8]
                    far_m[at, :] = m_all[8 * c:8 * c + 8]
        return carry

    lax.fori_loop(0, STRIDE // 2, far_step, 0)

    def mid_step(b, carry):
        which = 2 + jnp.where(b == 0, first_row, 0)
        for rho in range(4):
            rows_q = pl.ds(pl.multiple_of(far_rows * b, far_rows), far_rows)
            rows_k = pl.ds(pl.multiple_of(far_rows * (b + halo - 1), far_rows), 2 * far_rows)
            q = jnp.concatenate([q_far[rho + 4 * s, rows_q, :] for s in range(4)], axis=0)
            keys = jnp.concatenate([k_far[rho + 4 * s, rows_k, :] for s in range(4)], axis=0)
            keys1 = jnp.concatenate([k_far1[rho + 4 * s, rows_k, :] for s in range(4)], axis=0)
            w, m = scores(q, keys, which)
            res = jnp.dot(w, keys1, preferred_element_type=F32)
            m_all = jnp.broadcast_to(m, (LANES, LANES))
            for c in range(LANES // 8):
                at = pl.ds(pl.multiple_of(b * block + (c % 4) * LANES + 8 * (rho + 4 * (c // 4)), 8), 8)
                mid_r[at, :] = res[8 * c:8 * c + 8]
                mid_m[at, :] = m_all[8 * c:8 * c + 8]
        return carry

    lax.fori_loop(0, group, mid_step, 0)

    def o_copy(d, source):
        return pltpu.make_async_remote_copy(
            src_ref=o_send.at[d], dst_ref=o_recv.at[source],
            send_sem=o_s.at[d], recv_sem=o_r.at[source], device_id=peer(d), device_id_type=MESH)

    def l_copy(d, source):
        return pltpu.make_async_remote_copy(
            src_ref=l_send.at[d], dst_ref=l_recv.at[source],
            send_sem=l_s.at[d], recv_sem=l_r.at[source], device_id=peer(d), device_id_type=MESH)

    square_low = iota((LANES, LANES), 1) < HEAD_DIM
    eye = iota((LANES, LANES), 0) == iota((LANES, LANES), 1)

    def near_step(i, carry):
        b = lax.rem(x + i + group // 2, group)
        for a2 in range(2):
            pieces = []
            for a in (a2, a2 + 2):
                at = pl.ds(pl.multiple_of(b * block + a * LANES, LANES), LANES)
                keys = pl.ds(pl.multiple_of(REACH + b * block + (a - 1) * LANES, LANES), 2 * LANES)
                w, m = scores(q_near[at, :], kv[keys, :], jnp.where(b == 0, first_row, 0) if a == 0 else 0)
                res = jnp.dot(w, kv1[keys, :], preferred_element_type=F32)
                m_f, m_m = far_m[at, :], mid_m[at, :]
                top = jnp.maximum(jnp.maximum(m_f, m_m), m)
                den = jnp.exp(m - top) * res + jnp.exp(m_f - top) * far_r[at, :] + jnp.exp(m_m - top) * mid_r[at, :]
                turned = pltpu.roll(den, HEAD_DIM, 1)
                total = jnp.where(square_low, den, turned)
                l_send[b, a, :] = jnp.sum(jnp.where(eye, top + jnp.log(total), 0.0), axis=0)
                pieces.append((turned if a < 2 else den) / total)
            o_send[b, pl.ds(a2 * LANES, LANES), :] = jnp.where(square_low, pieces[0], pieces[1]).astype(BF16)

        @pl.when(b != x)
        def _():
            o_copy(b, x).start()
            l_copy(b, x).start()

        return carry

    lax.fori_loop(0, group, near_step, 0)
    own_o = pltpu.make_async_copy(o_send.at[x], o_recv.at[x], o_s.at[x])
    own_l = pltpu.make_async_copy(l_send.at[x], l_recv.at[x], l_s.at[x])
    own_o.start()
    own_l.start()
    own_o.wait()
    own_l.wait()

    def returned(i, carry):
        b = lax.rem(x + i, group)
        o_copy(b, b).wait_recv()
        l_copy(b, b).wait_recv()
        return carry

    lax.fori_loop(1, group, returned, 0)

    for p in range(group // 2):
        even, odd = o_recv[2 * p].astype(F32), o_recv[2 * p + 1].astype(F32)
        cols = slice(p * LANES, (p + 1) * LANES)
        first = jnp.where(low, even, pltpu.roll(odd, HEAD_DIM, 1)).astype(BF16)
        second = jnp.where(low, pltpu.roll(even, HEAD_DIM, 1), odd).astype(BF16)
        hid[:half, cols] = jnp.dot(back, first, preferred_element_type=F32).astype(BF16)
        hid[half:, cols] = jnp.dot(back, second, preferred_element_type=F32).astype(BF16)
    loads[4].wait()

    pieces_out = part.shape[0]
    step_cols = depth // pieces_out

    def part_copy(i):
        return pltpu.make_async_remote_copy(
            src_ref=part.at[i], dst_ref=other.at[i], send_sem=part_s.at[i], recv_sem=part_r.at[i],
            device_id=partner, device_id_type=MESH)

    for i in range(pieces_out):
        part[i] = jnp.dot(hid[pl.ds(other_half, half), :], o_w[:, i * step_cols:(i + 1) * step_cols],
                          preferred_element_type=F32).astype(BF16)
        part_copy(i).start()

    flat = jnp.concatenate([l_recv[h] for h in range(group)], axis=0)
    l_nat[...] = jnp.dot(flat, perm[:LANES, :LANES].astype(F32), preferred_element_type=F32, precision=lax.Precision.HIGHEST)
    for a in range(block // LANES):
        logs[:, a * LANES:(a + 1) * LANES] = l_nat[pl.ds(a, group, stride=8), :]

    for i in range(pieces_out):
        own = jnp.dot(hid[pl.ds(mine, half), :], o_w[:, i * step_cols:(i + 1) * step_cols],
                      preferred_element_type=F32).astype(BF16)
        part_copy(i).wait_recv()
        mixed[:, i * step_cols:(i + 1) * step_cols] = (own.astype(F32) + other[i].astype(F32)).astype(BF16)

    tok_copy.wait_send()
    for d in range(group):
        @pl.when(d != x)
        def _():
            kv_copy(d, x).wait_send()
            q_copy(d, x).wait_send()
            o_copy(d, x).wait_send()
            l_copy(d, x).wait_send()

    for i in range(halo):
        @pl.when(y < up)
        def _():
            halo_copy(i + group - halo).wait_send()

    for i in range(pieces_out):
        part_copy(i).wait_send()


def solution(mesh):
    def body(tokens, w_query, w_key, w_value, w_out):
        half, depth = tokens.shape
        width = w_query.shape[1]
        block, group = 2 * half, width // HEAD_DIM
        halo = REACH // block
        length = group * block
        far_rows = block // STRIDE
        pieces_out = 4
        vmem = pltpu.VMEM
        dma = pltpu.SemaphoreType.DMA
        anywhere = pl.BlockSpec(memory_space=pl.ANY)
        return pl.pallas_call(
            functools.partial(kernel, mesh.shape["sp"] // group),
            name="attention_layer",
            out_shape=(
                jax.ShapeDtypeStruct((half, depth), BF16),
                jax.ShapeDtypeStruct((group, block), F32),
            ),
            in_specs=[anywhere] * 5,
            out_specs=(pl.BlockSpec(memory_space=vmem), pl.BlockSpec(memory_space=vmem)),
            scratch_shapes=[
                vmem((block, depth), BF16),
                vmem((block, depth), BF16),
                vmem((depth, width), BF16),
                vmem((depth, width), BF16),
                vmem((depth, width), BF16),
                vmem((width, depth), BF16),
                vmem((block, 2 * LANES), F32),
                vmem((group, block, LANES), BF16),
                vmem((group, half, LANES), BF16),
                vmem((REACH + length, LANES), BF16),
                vmem((REACH + length, LANES), BF16),
                vmem((group, half, LANES), BF16),
                vmem((length, LANES), BF16),
                vmem((STRIDE, group * far_rows, LANES), BF16),
                vmem((STRIDE, (halo + group) * far_rows, LANES), BF16),
                vmem((STRIDE, (halo + group) * far_rows, LANES), BF16),
                vmem((6, LANES, 2 * LANES), F32),
                vmem((length, LANES), F32),
                vmem((length, LANES), F32),
                vmem((length, LANES), F32),
                vmem((length, LANES), F32),
                vmem((group, half, LANES), BF16),
                vmem((group, half, LANES), BF16),
                vmem((group, 8, LANES), F32),
                vmem((group, 8, LANES), F32),
                vmem((group * 8, LANES), F32),
                vmem((block, width), BF16),
                vmem((pieces_out, half, depth // pieces_out), BF16),
                vmem((pieces_out, half, depth // pieces_out), BF16),
                dma((5,)), dma((2,)),
                dma((group,)), dma((group,)), dma((group,)), dma((group,)),
                dma((halo,)), dma((halo,)),
                dma((group,)), dma((group,)), dma((group,)), dma((group,)),
                dma((pieces_out,)), dma((pieces_out,)),
                pltpu.SemaphoreType.REGULAR((group,)),
            ],
            compiler_params=pltpu.CompilerParams(
                collective_id=0, has_side_effects=True, vmem_limit_bytes=60 * 1024 * 1024
            ),
        )(tokens, w_query, w_key, w_value, w_out)

    in_specs = (
        P(("grp", "sp", "tp"), None),
        P(None, "tp"),
        P(None, "tp"),
        P(None, "tp"),
        P("tp", None),
    )
    out_specs = (P(("grp", "sp", "tp"), None), P("tp", ("grp", "sp")))
    return jax.shard_map(body, mesh=mesh, in_specs=in_specs, out_specs=out_specs, check_vma=False)
```

time: 259 us -> 93.7 us (0.36)
  the two profiles are of different devices: /device:TPU:513 before, /device:TPU:621 now
where the time goes in v1:
time: 93.7 us; the launch traced here: 93.6 us
  Pallas kernels  90 us (96%)
  local copies, waits for them, and re-layouts  2.92 us (3%)
    pallas_call x1, Pallas kernels, body(): pl.pallas_call(functools.partial(kernel, mesh.shape['sp'] // group), name...  90 us
    unnamed x4, local copies, waits for them, and re-layouts  2.92 us

profile of v1, /device:TPU:621, one launch (start us, length us, event | category | flops | bytes accessed | tf_op | source)
XLA Modules:
  0.0 93.6 jit_solution(9778303099337958491)
XLA Ops:
  0.6 90.0 %attention_layer.1 = (bf16[256,2048]{1,0:T(8,128)(2,1)}, f32[8,512]{1,0:T(8,128)}) custom-call(bf16[256,2048]{1,0:T(8,128)(2,1)} %tok.1, bf16[2048,512]{1,0:T(8,128)(2,1)} %wq.1, bf16[2048,512]{1,0:T(8,128)(2,1)} %wk.1, bf16[2048,512]{1,0:T(8,128)(2,1)} %wv.1, bf16[512,2048]{1,0:T(8,128)(2,1)} %wo.1), custom_call_target="tpu_custom_call" | custom-call | tf_op jit(solution)/shard_map/attention_layer/pallas_call | solution.py:399
  90.7 0.0 copy-start
  90.7 2.3 %copy.9 = bf16[256,2048]{1,0:T(8,128)(2,1)} copy(bf16[256,2048]{1,0:T(8,128)(2,1)} %get-tuple-element.4) | data formatting | bytes 2097152
  93.0 0.0 copy-done
  93.0 0.6 copy.10
Async XLA Ops:
  90.7 2.3 %copy-start = (f32[8,512]{1,0:T(8,128)S(1)}, f32[8,512]{1,0:T(8,128)}, u32[]{:S(2)}) copy-start(f32[8,512]{1,0:T(8,128)} %get-tuple-element.5) | copy-start | bytes 49156

commit v2 on v1

v2 whole, which is shorter than its diff:
```python
import functools

import jax
import jax.numpy as jnp
from jax import lax
from jax.experimental import pallas as pl
from jax.experimental.pallas import tpu as pltpu
from jax.sharding import PartitionSpec as P

HEADS = 16
HEAD_DIM = 64
STEPS = 128
REACH = 2048
ALIBI_EXP = 16.0
STRIDE = 16
LANES = 128
MASKED = -1e30
MESH = pl.DeviceIdType.MESH
F32 = jnp.float32
BF16 = jnp.bfloat16


def iota(shape, dim):
    return lax.broadcasted_iota(jnp.int32, shape, dim)


def permuted(m):
    return (m // LANES) * LANES + (m % 8) * STRIDE + (m % LANES) // 8


def kernel(
    rows_sp, tok, wq, wk, wv, wo, own_out, their_out, logs,
    x_in, x_perm, q_w, k_w, v_w, o_w, k_tmp, send_kv, send_q, kv, kv1, q_pk, q_near, q_far, k_far, k_far1,
    bias, far_r, far_m, mid_r, mid_m, o_send, o_recv, l_send, l_recv, l_nat, hid, part, own,
    load_sem, tok_sem, kv_s, kv_r, q_s, q_r, halo_s, halo_r, o_s, o_r, l_s, l_r, part_s, part_r, own_s,
    in_sem, pair_sem, row_sem,
):
    half, depth = tok.shape
    block = 2 * half
    group = q_w.shape[1] // HEAD_DIM
    halo = REACH // block
    far_rows = block // STRIDE
    tile = LANES // far_rows
    tiles = group // tile
    sp, tp = lax.axis_index("sp"), lax.axis_index("tp")
    x = lax.rem(sp, group)
    base = sp - x
    y = sp // group
    up = rows_sp - 1

    def peer(d):
        return {"sp": base + d, "tp": tp}

    partner = {"tp": 1 - tp}

    mine = pl.multiple_of(tp * half, half)
    other_half = pl.multiple_of((1 - tp) * half, half)
    loads = [
        pltpu.make_async_copy(tok, x_in.at[pl.ds(mine, half)], load_sem.at[0]),
        pltpu.make_async_copy(wk, k_w, load_sem.at[1]),
        pltpu.make_async_copy(wv, v_w, load_sem.at[2]),
        pltpu.make_async_copy(wq, q_w, load_sem.at[3]),
        pltpu.make_async_copy(wo, o_w, load_sem.at[4]),
    ]
    for c in loads:
        c.start()

    barrier = pltpu.get_barrier_semaphore()

    @pl.when(tp == 0)
    def _():
        pl.semaphore_signal(barrier, inc=1, device_id=partner, device_id_type=MESH)
        pl.semaphore_wait(pair_sem, 1)
        for d in range(group):
            @pl.when(d < x)
            def _():
                pl.semaphore_signal(barrier, inc=1, device_id=peer(d), device_id_type=MESH)

        @pl.when(y > 0)
        def _():
            pl.semaphore_signal(barrier, inc=1, device_id={"sp": sp - group}, device_id_type=MESH)

    @pl.when(tp == 1)
    def _():
        pl.semaphore_wait(barrier, 1)
        pl.semaphore_signal(pair_sem, inc=1, device_id=partner, device_id_type=MESH)

    loads[0].wait()
    tok_copy = pltpu.make_async_remote_copy(
        src_ref=x_in.at[pl.ds(mine, half)], dst_ref=x_in.at[pl.ds(mine, half)],
        send_sem=tok_sem.at[0], recv_sem=tok_sem.at[1], device_id=partner, device_id_type=MESH)
    tok_copy.start()
    pm, pt = iota((half, half), 0), iota((half, half), 1)
    perm = jnp.where(permuted(pm) == pt, 1.0, 0.0).astype(BF16)
    back = jnp.where(permuted(pt) == pm, 1.0, 0.0).astype(BF16)
    low = iota((half, LANES), 1) < HEAD_DIM
    low_square = iota((LANES, LANES), 1) < HEAD_DIM
    wide = 2 * LANES
    at_once = wide // HEAD_DIM

    def permute(first):
        x_perm[pl.ds(first, half), :] = jnp.dot(perm, x_in[pl.ds(first, half), :], preferred_element_type=F32).astype(BF16)

    def project_kv(first, g):
        rows, cols = pl.ds(first, half), slice(g * wide, (g + 1) * wide)
        k_tmp[...] = jnp.dot(x_perm[rows, :], k_w[:, cols], preferred_element_type=F32)
        v_all = jnp.dot(x_perm[rows, :], v_w[:, cols], preferred_element_type=F32)
        for p in range(2):
            k_p, v_p = k_tmp[:, p * LANES:(p + 1) * LANES], v_all[:, p * LANES:(p + 1) * LANES]
            d = g * at_once + 2 * p
            send_kv[d, rows, :] = jnp.where(low, k_p, pltpu.roll(v_p, HEAD_DIM, 1)).astype(BF16)
            send_kv[d + 1, rows, :] = jnp.where(low, pltpu.roll(k_p, HEAD_DIM, 1), v_p).astype(BF16)

    def project_q(first, g):
        cols = slice(g * wide, (g + 1) * wide)
        rows = pl.ds(pl.multiple_of(first // 2, LANES), LANES)
        q_all = jnp.dot(x_perm[pl.ds(first, half), :], q_w[:, cols], preferred_element_type=F32) * HEAD_DIM ** -0.5
        for p in range(2):
            q_a, q_b = q_all[:LANES, p * LANES:(p + 1) * LANES], q_all[LANES:, p * LANES:(p + 1) * LANES]
            d = g * at_once + 2 * p
            send_q[d, rows, :] = jnp.where(low_square, q_a, pltpu.roll(q_b, HEAD_DIM, 1)).astype(BF16)
            send_q[d + 1, rows, :] = jnp.where(low_square, pltpu.roll(q_a, HEAD_DIM, 1), q_b).astype(BF16)

    def meet_row():
        @pl.when(tp == 0)
        def _():
            greeted = group - 1 - x + jnp.where(y < up, 1, 0)

            @pl.when(greeted > 0)
            def _():
                pl.semaphore_wait(barrier, greeted)

            pl.semaphore_signal(row_sem, inc=1, device_id=partner, device_id_type=MESH)

        @pl.when(tp == 1)
        def _():
            pl.semaphore_wait(row_sem, 1)

        def tell(d, carry):
            pl.semaphore_signal(in_sem.at[x], inc=1, device_id=peer(d), device_id_type=MESH)
            return carry

        lax.fori_loop(x + 1, group, tell, 0)

    pl.when(y == 0)(meet_row)
    permute(mine)
    loads[1].wait()
    loads[2].wait()
    groups = list(reversed(range(group // at_once)))
    for g in groups:
        project_kv(mine, g)

    their_copy = pltpu.make_async_remote_copy(
        src_ref=x_in.at[pl.ds(mine, half)], dst_ref=x_in.at[pl.ds(other_half, half)],
        send_sem=tok_sem.at[0], recv_sem=tok_sem.at[1], device_id=partner, device_id_type=MESH)
    their_copy.wait_recv()
    permute(other_half)

    def kv_copy(d, source):
        return pltpu.make_async_remote_copy(
            src_ref=send_kv.at[d], dst_ref=kv.at[pl.ds(pl.multiple_of(REACH + source * block, block), block)],
            send_sem=kv_s.at[d], recv_sem=kv_r.at[source], device_id=peer(d), device_id_type=MESH)

    def q_copy(d, source):
        return pltpu.make_async_remote_copy(
            src_ref=send_q.at[d], dst_ref=q_pk.at[source],
            send_sem=q_s.at[d], recv_sem=q_r.at[source], device_id=peer(d), device_id_type=MESH)

    own_kv = pltpu.make_async_copy(send_kv.at[x], kv.at[pl.ds(pl.multiple_of(REACH + x * block, block), block)], kv_s.at[x])
    own_q = pltpu.make_async_copy(send_q.at[x], q_pk.at[x], q_s.at[x])

    def offset(i):
        return jnp.where(lax.rem(i, 2) == 1, (i + 1) // 2, group - i // 2)

    def late(d):
        return (d == 0) & (y == 0)

    for n, g in enumerate(groups):
        project_kv(other_half, g)
        if n == 0:
            pl.when(y > 0)(meet_row)

        def send_keys(i, carry):
            d = lax.rem(x + offset(i), group)

            @pl.when((d // at_once == g) & ~late(d))
            def _():
                @pl.when(d < x)
                def _():
                    pl.semaphore_wait(in_sem.at[d], 1)

                kv_copy(d, x).start()

            return carry

        lax.fori_loop(1, group, send_keys, 0)

        @pl.when(x // at_once == g)
        def _():
            own_kv.start()

    loads[3].wait()
    for g in groups:
        project_q(mine, g)
        project_q(other_half, g)
    own_q.start()

    @pl.when((x > 0) & late(0))
    def _():
        pl.semaphore_wait(in_sem.at[0], 1)
        kv_copy(0, x).start()

    def send_queries(i, carry):
        d = lax.rem(x + offset(i), group)

        q_copy(d, x).start()
        return carry

    lax.fori_loop(1, group, send_queries, 0)

    head = (tp * group + x + 1).astype(F32)
    slope = jnp.exp2(jnp.full((LANES, 2 * LANES), -ALIBI_EXP / HEADS, F32) * head)
    row, col = iota((LANES, 2 * LANES), 0), iota((LANES, 2 * LANES), 1)
    near_d = STEPS + permuted(row) - (col // LANES) * LANES - permuted(col % LANES)
    mid_d = STEPS + 4 * (row % 32) + row // 32 - ((col % 64) // 32) * LANES - 4 * (col % 32) - col // 64
    far_d = STEPS + row - col
    before = (col < LANES, (col % 64) < 32, col < LANES)
    for w, (dist, stride) in enumerate(((near_d, 1), (mid_d, 4), (far_d, 16))):
        plain = jnp.where((dist >= 0) & (dist <= STEPS), -slope * (dist * stride).astype(F32), MASKED)
        bias[2 * w] = plain
        bias[2 * w + 1] = jnp.where(before[w] & (y == 0), MASKED, plain)

    @pl.when(y == 0)
    def _():
        kv[pl.ds(0, REACH), :] = jnp.zeros((REACH, LANES), BF16)

    def to_far(ref, first, second, slot, part_index):
        for r in range(STRIDE):
            pair = jnp.concatenate([first[8 * r:8 * r + 8], second[8 * r:8 * r + 8]], axis=0)
            ref[r, pl.ds(pl.multiple_of(far_rows * slot + 16 * part_index, 16), 16), :] = pair.astype(BF16)

    def take_keys(slot):
        for h in range(2):
            first = pl.multiple_of(slot * block + h * half, half)
            values = kv[pl.ds(first, half), :].astype(F32)
            with_ones = jnp.where(low, 1.0, values)
            kv1[pl.ds(first, half), :] = with_ones.astype(BF16)
            to_far(k_far, values[:LANES], values[LANES:], slot, h)
            to_far(k_far1, with_ones[:LANES], with_ones[LANES:], slot, h)

    def take_queries(b):
        for h in range(2):
            values = q_pk[b, h * LANES:(h + 1) * LANES, :].astype(F32)
            first = jnp.where(low_square, values, 0.0)
            second = jnp.where(low_square, pltpu.roll(values, HEAD_DIM, 1), 0.0)
            at = pl.multiple_of(b * block + h * half, half)
            q_near[pl.ds(at, LANES), :] = first.astype(BF16)
            q_near[pl.ds(at + LANES, LANES), :] = second.astype(BF16)
            to_far(q_far, first, second, b, h)

    def halo_copy(b):
        return pltpu.make_async_remote_copy(
            src_ref=kv.at[pl.ds(pl.multiple_of(REACH + b * block, block), block)],
            dst_ref=kv.at[pl.ds(pl.multiple_of((b - (group - halo)) * block, block), block)],
            send_sem=halo_s.at[b - (group - halo)], recv_sem=halo_r.at[b - (group - halo)],
            device_id={"sp": sp + group, "tp": tp}, device_id_type=MESH)

    def pass_on(b):
        @pl.when((b >= group - halo) & (y < up))
        def _():
            halo_copy(b).start()

    own_kv.wait()
    pass_on(x)
    take_keys(x + halo)
    own_q.wait()

    def arrive(i, carry):
        b = lax.rem(x + offset(i), group)

        @pl.when(~late(b))
        def _():
            kv_copy(b, b).wait_recv()
            pass_on(b)
            take_keys(b + halo)

        return carry

    lax.fori_loop(1, group, arrive, 0)

    @pl.when((x > 0) & late(0))
    def _():
        kv_copy(0, 0).wait_recv()
        take_keys(halo)


    def take_halo(i, carry):
        @pl.when(y > 0)
        def _():
            halo_copy(i + group - halo).wait_recv()

        take_keys(i)
        return carry

    def scores(q, keys, which):
        s = lax.dot_general(q, keys, (((1,), (1,)), ((), ())), preferred_element_type=F32) + bias[which]
        m = jnp.max(s, axis=1, keepdims=True)
        return jnp.exp(s - m).astype(BF16), m

    first_row = jnp.where(y == 0, 1, 0)
    eye = iota((LANES, LANES), 0) == iota((LANES, LANES), 1)

    def mid_step(b):
        which = 2 + jnp.where(b == 0, first_row, 0)
        rows_q = pl.ds(pl.multiple_of(far_rows * b, far_rows), far_rows)
        rows_k = pl.ds(pl.multiple_of(far_rows * (b + halo - 1), far_rows), 2 * far_rows)
        for rho in range(4):
            q = jnp.concatenate([q_far[rho + 4 * s, rows_q, :] for s in range(4)], axis=0)
            keys = jnp.concatenate([k_far[rho + 4 * s, rows_k, :] for s in range(4)], axis=0)
            keys1 = jnp.concatenate([k_far1[rho + 4 * s, rows_k, :] for s in range(4)], axis=0)
            w, m = scores(q, keys, which)
            res = jnp.dot(w, keys1, preferred_element_type=F32)
            m_all = jnp.broadcast_to(m, (LANES, LANES))
            for c in range(LANES // 8):
                at = pl.ds(pl.multiple_of(b * block + (c % 4) * LANES + 8 * (rho + 4 * (c // 4)), 8), 8)
                mid_r[at, :] = res[8 * c:8 * c + 8]
                mid_m[at, :] = m_all[8 * c:8 * c + 8]

    def o_copy(d, source):
        return pltpu.make_async_remote_copy(
            src_ref=o_send.at[d], dst_ref=o_recv.at[source],
            send_sem=o_s.at[d], recv_sem=o_r.at[source], device_id=peer(d), device_id_type=MESH)

    def l_copy(d, source):
        return pltpu.make_async_remote_copy(
            src_ref=l_send.at[d], dst_ref=l_recv.at[source],
            send_sem=l_s.at[d], recv_sem=l_r.at[source], device_id=peer(d), device_id_type=MESH)

    def near_step(b):
        for a in range(block // LANES):
            at = pl.ds(pl.multiple_of(b * block + a * LANES, LANES), LANES)
            keys = pl.ds(pl.multiple_of(REACH + b * block + (a - 1) * LANES, LANES), 2 * LANES)
            w, m = scores(q_near[at, :], kv[keys, :], jnp.where(b == 0, first_row, 0) if a == 0 else 0)
            res = jnp.dot(w, kv1[keys, :], preferred_element_type=F32)
            m_m = mid_m[at, :]
            top = jnp.maximum(m_m, m)
            mid_r[at, :] = jnp.exp(m - top) * res + jnp.exp(m_m - top) * mid_r[at, :]
            mid_m[at, :] = top

    def finish(b):
        for h in range(2):
            pieces = []
            for a in (2 * h, 2 * h + 1):
                at = pl.ds(pl.multiple_of(b * block + a * LANES, LANES), LANES)
                m_f, m_m = far_m[at, :], mid_m[at, :]
                top = jnp.maximum(m_f, m_m)
                den = jnp.exp(m_f - top) * far_r[at, :] + jnp.exp(m_m - top) * mid_r[at, :]
                turned = pltpu.roll(den, HEAD_DIM, 1)
                total = jnp.where(low_square, den, turned)
                l_send[b, a, :] = jnp.sum(jnp.where(eye, top + jnp.log(total), 0.0), axis=0)
                pieces.append((den if a % 2 else turned) / total)
            o_send[b, pl.ds(h * LANES, LANES), :] = jnp.where(low_square, pieces[0], pieces[1]).astype(BF16)

        @pl.when(b != x)
        def _():
            o_copy(b, x).start()
            l_copy(b, x).start()

    def far_tile(which_tile):
        first_q = pl.multiple_of(which_tile * LANES, LANES)
        which = 4 + jnp.where(which_tile == 0, first_row, 0)

        def far_step(i, c0):
            for rr in range(8):
                r = 8 * i + rr
                w, m = scores(q_far[r, pl.ds(first_q, LANES), :], k_far[r, pl.ds(first_q, 2 * LANES), :], which)
                res = jnp.dot(w, k_far1[r, pl.ds(first_q, 2 * LANES), :], preferred_element_type=F32)
                m_all = jnp.broadcast_to(m, (LANES, LANES))
                for c in range(LANES // 8):
                    at = pl.ds(pl.multiple_of((which_tile * tile + c // 4) * block + (c % 4) * LANES + 8 * r, 8), 8)
                    far_r[at, :] = res[8 * c:8 * c + 8]
                    far_m[at, :] = m_all[8 * c:8 * c + 8]
            return c0

        lax.fori_loop(0, STRIDE // 8, far_step, 0)

    def close(which_tile):
        far_tile(which_tile)

        def finish_one(j, c):
            finish(which_tile * tile + lax.rem(x + 1 + j, tile))
            return c

        lax.fori_loop(0, tile, finish_one, 0)

    def near_and_mid(b):
        mid_step(b)
        near_step(b)

    def queries(i, carry):
        b = lax.rem(x + jnp.where(i == 0, 0, offset(i)), group)

        @pl.when(b != x)
        def _():
            q_copy(b, b).wait_recv()

        take_queries(b)
        pl.when(b > 0)(lambda: near_and_mid(b))
        return carry

    lax.fori_loop(0, group, queries, 0)

    def close_tile(t, carry):
        which_tile = tiles - 1 - t

        @pl.when(which_tile == 0)
        def _():
            lax.fori_loop(0, halo, take_halo, 0)
            near_and_mid(0)

        close(which_tile)
        return carry

    lax.fori_loop(0, tiles, close_tile, 0)
    own_o = pltpu.make_async_copy(o_send.at[x], o_recv.at[x], o_s.at[x])
    own_l = pltpu.make_async_copy(l_send.at[x], l_recv.at[x], l_s.at[x])
    own_o.start()
    own_l.start()
    own_o.wait()
    own_l.wait()
    loads[4].wait()

    def returned(i, carry):
        b = lax.rem(x + offset(i), group)
        o_copy(b, b).wait_recv()
        l_copy(b, b).wait_recv()
        return carry

    lax.fori_loop(1, group, returned, 0)

    for p in range(group // 2):
        cols = slice(p * LANES, (p + 1) * LANES)
        for h in range(2):
            rows = slice(h * LANES, (h + 1) * LANES)
            even, odd = o_recv[2 * p, rows, :].astype(F32), o_recv[2 * p + 1, rows, :].astype(F32)
            both = jnp.concatenate([jnp.where(low_square, even, pltpu.roll(odd, HEAD_DIM, 1)),
                                    jnp.where(low_square, pltpu.roll(even, HEAD_DIM, 1), odd)], axis=0).astype(BF16)
            hid[h * half:(h + 1) * half, cols] = jnp.dot(back, both, preferred_element_type=F32).astype(BF16)

    pieces_out = part.shape[0]
    step_cols = depth // pieces_out

    def part_copy(i):
        return pltpu.make_async_remote_copy(
            src_ref=part.at[i], dst_ref=their_out.at[:, i * step_cols:(i + 1) * step_cols],
            send_sem=part_s.at[i], recv_sem=part_r.at[i], device_id=partner, device_id_type=MESH)

    def own_copy(i):
        return pltpu.make_async_copy(own.at[i], own_out.at[:, i * step_cols:(i + 1) * step_cols], own_s.at[i])

    for i in range(pieces_out):
        part[i] = jnp.dot(hid[pl.ds(other_half, half), :], o_w[:, i * step_cols:(i + 1) * step_cols],
                          preferred_element_type=F32).astype(BF16)
        part_copy(i).start()

    for i in range(pieces_out):
        own[i] = jnp.dot(hid[pl.ds(mine, half), :], o_w[:, i * step_cols:(i + 1) * step_cols],
                         preferred_element_type=F32).astype(BF16)
        own_copy(i).start()

    flat = jnp.concatenate([l_recv[h] for h in range(group)], axis=0)
    l_nat[...] = jnp.dot(flat, perm[:LANES, :LANES].astype(F32), preferred_element_type=F32, precision=lax.Precision.HIGHEST)
    for a in range(block // LANES):
        logs[:, a * LANES:(a + 1) * LANES] = l_nat[pl.ds(a, group, stride=8), :]

    tok_copy.wait_send()
    for d in range(group):
        @pl.when(d != x)
        def _():
            kv_copy(d, x).wait_send()
            q_copy(d, x).wait_send()
            o_copy(d, x).wait_send()
            l_copy(d, x).wait_send()

    for i in range(halo):
        @pl.when(y < up)
        def _():
            halo_copy(i + group - halo).wait_send()

    for i in range(pieces_out):
        own_copy(i).wait()
        part_copy(i).wait_recv()
        part_copy(i).wait_send()


def solution(mesh):
    def body(tokens, w_query, w_key, w_value, w_out):
        half, depth = tokens.shape
        width = w_query.shape[1]
        block, group = 2 * half, width // HEAD_DIM
        halo = REACH // block
        length = group * block
        far_rows = block // STRIDE
        pieces_out = 4
        vmem = pltpu.VMEM
        dma = pltpu.SemaphoreType.DMA
        anywhere = pl.BlockSpec(memory_space=pl.ANY)
        own, theirs, log_sums = pl.pallas_call(
            functools.partial(kernel, mesh.shape["sp"] // group),
            name="attention_layer",
            out_shape=(
                jax.ShapeDtypeStruct((half, depth), BF16),
                jax.ShapeDtypeStruct((half, depth), BF16),
                jax.ShapeDtypeStruct((group, block), F32),
            ),
            in_specs=[anywhere] * 5,
            out_specs=(anywhere, anywhere, pl.BlockSpec(memory_space=vmem)),
            scratch_shapes=[
                vmem((block, depth), BF16),
                vmem((block, depth), BF16),
                vmem((depth, width), BF16),
                vmem((depth, width), BF16),
                vmem((depth, width), BF16),
                vmem((width, depth), BF16),
                vmem((half, 2 * LANES), F32),
                vmem((group, block, LANES), BF16),
                vmem((group, half, LANES), BF16),
                vmem((REACH + length, LANES), BF16),
                vmem((REACH + length, LANES), BF16),
                vmem((group, half, LANES), BF16),
                vmem((length, LANES), BF16),
                vmem((STRIDE, group * far_rows, LANES), BF16),
                vmem((STRIDE, (halo + group) * far_rows, LANES), BF16),
                vmem((STRIDE, (halo + group) * far_rows, LANES), BF16),
                vmem((6, LANES, 2 * LANES), F32),
                vmem((length, LANES), F32),
                vmem((length, LANES), F32),
                vmem((length, LANES), F32),
                vmem((length, LANES), F32),
                vmem((group, half, LANES), BF16),
                vmem((group, half, LANES), BF16),
                vmem((group, 8, LANES), F32),
                vmem((group, 8, LANES), F32),
                vmem((group * 8, LANES), F32),
                vmem((block, width), BF16),
                vmem((pieces_out, half, depth // pieces_out), BF16),
                vmem((pieces_out, half, depth // pieces_out), BF16),
                dma((5,)), dma((2,)),
                dma((group,)), dma((group,)), dma((group,)), dma((group,)),
                dma((halo,)), dma((halo,)),
                dma((group,)), dma((group,)), dma((group,)), dma((group,)),
                dma((pieces_out,)), dma((pieces_out,)), dma((pieces_out,)),
                pltpu.SemaphoreType.REGULAR((group,)), pltpu.SemaphoreType.REGULAR, pltpu.SemaphoreType.REGULAR,
            ],
            compiler_params=pltpu.CompilerParams(
                collective_id=0, has_side_effects=True, vmem_limit_bytes=60 * 1024 * 1024
            ),
        )(tokens, w_query, w_key, w_value, w_out)
        return (own.astype(F32) + theirs.astype(F32)).astype(BF16), log_sums

    in_specs = (
        P(("grp", "sp", "tp"), None),
        P(None, "tp"),
        P(None, "tp"),
        P(None, "tp"),
        P("tp", None),
    )
    out_specs = (P(("grp", "sp", "tp"), None), P("tp", ("grp", "sp")))
    return jax.shard_map(body, mesh=mesh, in_specs=in_specs, out_specs=out_specs, check_vma=False)
```

time: 93.7 us -> 78.4 us (0.84)
  the two profiles are of different devices: /device:TPU:621 before, /device:TPU:513 now
where the time goes in v2:
time: 78.4 us; the launch traced here: 78.2 us
  Pallas kernels  74.1 us (95%)
  other arithmetic  2.91 us (4%)
    pallas_call x1, Pallas kernels, body(): pl.pallas_call(functools.partial(kernel, mesh.shape['sp'] // group), name...  74.1 us
    convert_element_type x1, other arithmetic, body(): return ((own.astype(F32) + theirs.astype(F32)).astype(BF16), log_sums)  2.91 us

profile of v2, /device:TPU:513, one launch (start us, length us, event | category | flops | bytes accessed | tf_op | source)
XLA Modules:
  0.0 78.2 jit_solution(3861439025695599295)
XLA Ops:
  0.6 74.1 %attention_layer.1 = (bf16[256,2048]{1,0:T(8,128)(2,1)}, bf16[256,2048]{1,0:T(8,128)(2,1)}, f32[8,512]{1,0:T(8,128)}) custom-call(bf16[256,2048]{1,0:T(8,128)(2,1)} %tok.1, bf16[2048,512]{1,0:T(8,128)(2,1)} %wq.1, bf16[2048,512]{1,0:T(8,128)(2,1)} %wk.1, bf16[2048,512]{1,0:T(8,128)(2,1)} %wv.1, bf16[512,2048]{1,0:T(8,128)(2,1)} %wo.1), custom_call_target="tpu_custom_call" | custom-call | tf_op jit(solution)/shard_map/attention_layer/pallas_call | solution.py:508
  74.7 0.0 copy-start
  74.7 2.9 %add_convert_fusion = bf16[256,2048]{1,0:T(8,128)(2,1)} fusion(bf16[256,2048]{1,0:T(8,128)(2,1)} %get-tuple-element.6, bf16[256,2048]{1,0:T(8,128)(2,1)} %get-tuple-element.5), kind=kLoop, calls=%fused_computation | loop fusion | flops 2097152 | bytes 3145728 | tf_op jit(solution)/shard_map/convert_element_type | solution.py:559
  77.6 0.0 copy-done
  77.6 0.6 copy.8
Async XLA Ops:
  74.7 2.9 %copy-start = (f32[8,512]{1,0:T(8,128)S(1)}, f32[8,512]{1,0:T(8,128)}, u32[]{:S(2)}) copy-start(f32[8,512]{1,0:T(8,128)} %get-tuple-element.11) | copy-start | bytes 49156

commit v3 on v2

--- a/solution.py
+++ b/solution.py
@@ -143,30 +143,18 @@
         lax.fori_loop(x + 1, group, tell, 0)
 
     pl.when(y == 0)(meet_row)
-    permute(mine)
-    loads[1].wait()
-    loads[2].wait()
-    groups = list(reversed(range(group // at_once)))
-    for g in groups:
-        project_kv(mine, g)
-
-    their_copy = pltpu.make_async_remote_copy(
-        src_ref=x_in.at[pl.ds(mine, half)], dst_ref=x_in.at[pl.ds(other_half, half)],
-        send_sem=tok_sem.at[0], recv_sem=tok_sem.at[1], device_id=partner, device_id_type=MESH)
-    their_copy.wait_recv()
-    permute(other_half)
-
-    def kv_copy(d, source):
+    def kv_copy(d, source, h):
         return pltpu.make_async_remote_copy(
-            src_ref=send_kv.at[d], dst_ref=kv.at[pl.ds(pl.multiple_of(REACH + source * block, block), block)],
-            send_sem=kv_s.at[d], recv_sem=kv_r.at[source], device_id=peer(d), device_id_type=MESH)
+            src_ref=send_kv.at[d, pl.ds(pl.multiple_of(h * half, half), half)],
+            dst_ref=kv.at[pl.ds(pl.multiple_of(REACH + source * block + h * half, half), half)],
+            send_sem=kv_s.at[2 * d + h], recv_sem=kv_r.at[2 * source + h], device_id=peer(d), device_id_type=MESH)
 
     def q_copy(d, source):
         return pltpu.make_async_remote_copy(
             src_ref=send_q.at[d], dst_ref=q_pk.at[source],
             send_sem=q_s.at[d], recv_sem=q_r.at[source], device_id=peer(d), device_id_type=MESH)
 
-    own_kv = pltpu.make_async_copy(send_kv.at[x], kv.at[pl.ds(pl.multiple_of(REACH + x * block, block), block)], kv_s.at[x])
+    own_kv = pltpu.make_async_copy(send_kv.at[x], kv.at[pl.ds(pl.multiple_of(REACH + x * block, block), block)], kv_s.at[2 * x])
     own_q = pltpu.make_async_copy(send_q.at[x], q_pk.at[x], q_s.at[x])
 
     def offset(i):
@@ -175,29 +163,39 @@
     def late(d):
         return (d == 0) & (y == 0)
 
-    for n, g in enumerate(groups):
+    def send_keys(h, first_time):
+        def one(i, carry):
+            d = lax.rem(x + offset(i), group)
+
+            @pl.when(~late(d))
+            def _():
+                if first_time:
+                    @pl.when(d < x)
+                    def _():
+                        pl.semaphore_wait(in_sem.at[d], 1)
+
+                kv_copy(d, x, h).start()
+
+            return carry
+
+        lax.fori_loop(1, group, one, 0)
+
+    permute(mine)
+    loads[1].wait()
+    loads[2].wait()
+    groups = range(group // at_once)
+    for g in groups:
+        project_kv(mine, g)
+    pl.when(y > 0)(meet_row)
+    send_keys(tp, True)
+    pltpu.make_async_remote_copy(
+        src_ref=x_in.at[pl.ds(mine, half)], dst_ref=x_in.at[pl.ds(other_half, half)],
+        send_sem=tok_sem.at[0], recv_sem=tok_sem.at[1], device_id=partner, device_id_type=MESH).wait_recv()
+    permute(other_half)
+    for g in groups:
         project_kv(other_half, g)
-        if n == 0:
-            pl.when(y > 0)(meet_row)
-
-        def send_keys(i, carry):
-            d = lax.rem(x + offset(i), group)
-
-            @pl.when((d // at_once == g) & ~late(d))
-            def _():
-                @pl.when(d < x)
-                def _():
-                    pl.semaphore_wait(in_sem.at[d], 1)
-
-                kv_copy(d, x).start()
-
-            return carry
-
-        lax.fori_loop(1, group, send_keys, 0)
-
-        @pl.when(x // at_once == g)
-        def _():
-            own_kv.start()
+    send_keys(1 - tp, False)
+    own_kv.start()
 
     loads[3].wait()
     for g in groups:
@@ -208,7 +206,8 @@
     @pl.when((x > 0) & late(0))
     def _():
         pl.semaphore_wait(in_sem.at[0], 1)
-        kv_copy(0, x).start()
+        kv_copy(0, x, tp).start()
+        kv_copy(0, x, 1 - tp).start()
 
     def send_queries(i, carry):
         d = lax.rem(x + offset(i), group)
@@ -280,18 +279,14 @@
 
         @pl.when(~late(b))
         def _():
-            kv_copy(b, b).wait_recv()
+            kv_copy(b, b, 0).wait_recv()
+            kv_copy(b, b, 1).wait_recv()
             pass_on(b)
             take_keys(b + halo)
 
         return carry
 
     lax.fori_loop(1, group, arrive, 0)
-
-    @pl.when((x > 0) & late(0))
-    def _():
-        kv_copy(0, 0).wait_recv()
-        take_keys(halo)
 
 
     def take_halo(i, carry):
@@ -400,22 +395,38 @@
     def queries(i, carry):
         b = lax.rem(x + jnp.where(i == 0, 0, offset(i)), group)
 
-        @pl.when(b != x)
-        def _():
-            q_copy(b, b).wait_recv()
-
-        take_queries(b)
-        pl.when(b > 0)(lambda: near_and_mid(b))
+        @pl.when((b == x) | ~late(b))
+        def _():
+            @pl.when(b != x)
+            def _():
+                q_copy(b, b).wait_recv()
+
+            take_queries(b)
+            pl.when((b > 0) & ((x == 0) | ~late(b - 1)))(lambda: near_and_mid(b))
+
         return carry
 
     lax.fori_loop(0, group, queries, 0)
 
+    @pl.when((x > 0) & late(0))
+    def _():
+        kv_copy(0, 0, 0).wait_recv()
+        kv_copy(0, 0, 1).wait_recv()
+        take_keys(halo)
+        near_and_mid(1)
+
     def close_tile(t, carry):
-        which_tile = tiles - 1 - t
+        which_tile = lax.rem(jnp.where((y == 1) & (x == 0), tiles - 1, 0) + t, tiles)
 
         @pl.when(which_tile == 0)
         def _():
             lax.fori_loop(0, halo, take_halo, 0)
+
+            @pl.when((x > 0) & late(0))
+            def _():
+                q_copy(0, 0).wait_recv()
+                take_queries(0)
+
             near_and_mid(0)
 
         close(which_tile)
@@ -477,7 +488,8 @@
     for d in range(group):
         @pl.when(d != x)
         def _():
-            kv_copy(d, x).wait_send()
+            kv_copy(d, x, 0).wait_send()
+            kv_copy(d, x, 1).wait_send()
             q_copy(d, x).wait_send()
             o_copy(d, x).wait_send()
             l_copy(d, x).wait_send()
@@ -513,7 +525,7 @@
                 jax.ShapeDtypeStruct((half, depth), BF16),
                 jax.ShapeDtypeStruct((group, block), F32),
             ),
-            in_specs=[anywhere] * 5,
+            in_specs=[pl.BlockSpec(memory_space=pltpu.MemorySpace.HBM)] * 5,
             out_specs=(anywhere, anywhere, pl.BlockSpec(memory_space=vmem)),
             scratch_shapes=[
                 vmem((block, depth), BF16),
@@ -546,14 +558,14 @@
                 vmem((pieces_out, half, depth // pieces_out), BF16),
                 vmem((pieces_out, half, depth // pieces_out), BF16),
                 dma((5,)), dma((2,)),
-                dma((group,)), dma((group,)), dma((group,)), dma((group,)),
+                dma((2 * group,)), dma((2 * group,)), dma((group,)), dma((group,)),
                 dma((halo,)), dma((halo,)),
                 dma((group,)), dma((group,)), dma((group,)), dma((group,)),
                 dma((pieces_out,)), dma((pieces_out,)), dma((pieces_out,)),
                 pltpu.SemaphoreType.REGULAR((group,)), pltpu.SemaphoreType.REGULAR, pltpu.SemaphoreType.REGULAR,
             ],
             compiler_params=pltpu.CompilerParams(
-                collective_id=0, has_side_effects=True, vmem_limit_bytes=60 * 1024 * 1024
+                collective_id=0, has_side_effects=True, vmem_limit_bytes=51 * 1024 * 1024
             ),
         )(tokens, w_query, w_key, w_value, w_out)
         return (own.astype(F32) + theirs.astype(F32)).astype(BF16), log_sums

time: 78.4 us -> 73.8 us (0.941)
  the two profiles are of different devices: /device:TPU:513 before, /device:TPU:527 now
where the time goes in v3:
time: 73.8 us; the launch traced here: 73.7 us
  Pallas kernels  71.1 us (96%)
  other arithmetic  1.36 us (2%)
    pallas_call x1, Pallas kernels, body(): pl.pallas_call(functools.partial(kernel, mesh.shape['sp'] // group), name...  71.1 us

profile of v3, /device:TPU:527, one launch (start us, length us, event | category | flops | bytes accessed | tf_op | source)
XLA Modules:
  0.0 73.7 jit_solution(9186521780391234749)
XLA Ops:
  0.6 71.1 %attention_layer.1 = (bf16[256,2048]{1,0:T(8,128)(2,1)S(1)}, bf16[256,2048]{1,0:T(8,128)(2,1)S(1)}, f32[8,512]{1,0:T(8,128)S(1)}) custom-call(bf16[256,2048]{1,0:T(8,128)(2,1)} %tok.1, bf16[2048,512]{1,0:T(8,128)(2,1)} %wq.1, bf16[2048,512]{1,0:T(8,128)(2,1)} %wk.1, bf16[2048,512]{1,0:T(8,128)(2,1)} %wv.1, bf16[512,2048]{1,0:T(8,128)(2,1)} %wo.1), custom_call_target="tpu_custom_call" | custom-call | tf_op jit(solution)/shard_map/attention_layer/pallas_call | solution.py:520
  71.7 1.4 %add_convert_fusion = bf16[256,2048]{1,0:T(8,128)(2,1)} fusion(bf16[256,2048]{1,0:T(8,128)(2,1)S(1)} %get-tuple-element.6, bf16[256,2048]{1,0:T(8,128)(2,1)S(1)} %get-tuple-element.5), kind=kLoop, calls=%fused_computation | loop fusion | flops 2097152 | bytes 3145728 | tf_op jit(solution)/shard_map/convert_element_type | solution.py:571
  73.1 0.6 copy.8
